TPU v7x, 32 devices: a whole 2x2x4 slice. The times are simulated.
32 devices in a mesh: gr: 2 (over x), fs: 8 (over z, y), tp: 2 (over core).
Axes of the slice: x: 2, y: 2, z: 4, core: 2. Of those that a mesh axis runs over, the one named last changes fastest.
Arguments:
- prompt: bfloat16 [3072, 2048], P(('gr', 'fs', 'tp')), may hold values from -6 to 6
- norm_first: float32 [2048], P(('gr', 'fs')), may hold values from 0.1 to 1.9
- gate_first: float32 [2048, 5632], P(('gr', 'fs'), 'tp'), may hold values from -6 to 6
- up_first: float32 [2048, 5632], P(('gr', 'fs'), 'tp'), may hold values from -6 to 6
- down_first: float32 [2048, 5632], P(('gr', 'fs'), 'tp'), may hold values from -6 to 6
- norm_second: float32 [2048], P(('gr', 'fs')), may hold values from 0.1 to 1.9
- gate_second: float32 [2048, 5632], P(('gr', 'fs'), 'tp'), may hold values from -6 to 6
- up_second: float32 [2048, 5632], P(('gr', 'fs'), 'tp'), may hold values from -6 to 6
- down_second: float32 [2048, 5632], P(('gr', 'fs'), 'tp'), may hold values from -6 to 6
Outputs:
- served_gate_first: bfloat16 [2048, 5632], P(None, 'fs')
- served_up_first: bfloat16 [2048, 5632], P(None, 'fs')
- served_down_first: bfloat16 [2048, 5632], P(None, 'fs')
- served_gate_second: bfloat16 [2048, 5632], P(None, 'fs')
- served_up_second: bfloat16 [2048, 5632], P(None, 'fs')
- served_down_second: bfloat16 [2048, 5632], P(None, 'fs')
- result: bfloat16 [3072, 2048], P(('gr', 'fs', 'tp'))
All inputs are finite; a program needn't handle non-finite values.
Results may differ from a plain program's by a relative error of at most 0.015.
Values may be sent and summed in bfloat16 or wider, within the bound.
A program may use at most 128 MiB of HBM per device.

v0:
```python
import jax
import jax.numpy as jnp
from jax import lax
from jax.sharding import PartitionSpec as P

D = 2048
FF = 5632
EPS = 1e-06


def fold_rows(gain, weight):
    return (gain[:, None] * weight).astype(jnp.bfloat16)


def relayout(stacked):
    moved = lax.all_to_all(
        lax.all_to_all(stacked, "tp", split_axis=1, concat_axis=2, tiled=True),
        "fs",
        split_axis=2,
        concat_axis=1,
        tiled=True,
    )
    whole = lax.all_gather(moved, ("gr", "tp"), axis=1, tiled=True)
    matrices = stacked.shape[0]
    block_width = moved.shape[2]
    gr_size = lax.axis_size("gr")
    tp_size = lax.axis_size("tp")
    fs_size = lax.axis_size("fs")
    sub_rows = stacked.shape[1] // tp_size
    shaped = whole.reshape(matrices, gr_size, tp_size, fs_size, sub_rows, block_width)
    return shaped.transpose(0, 1, 3, 2, 4, 5).reshape(
        matrices, gr_size * fs_size * tp_size * sub_rows, block_width
    )


def half_step(residual, weights):
    gate_weight = weights[0]
    up_weight = weights[1]
    down_weight = weights[2]
    resid_f = residual.astype(jnp.float32)
    normed = (
        resid_f * lax.rsqrt(jnp.mean(resid_f * resid_f, axis=-1, keepdims=True) + EPS)
    ).astype(jnp.bfloat16)
    in_scale = D ** (-0.5)
    out_scale = FF ** (-0.5)
    tokens_in = lax.all_gather(normed, "fs", axis=0, tiled=True)
    gate_pre = jnp.dot(tokens_in, gate_weight, preferred_element_type=jnp.float32) * in_scale
    up_pre = jnp.dot(tokens_in, up_weight, preferred_element_type=jnp.float32) * in_scale
    hidden = (jax.nn.silu(gate_pre) * up_pre).astype(jnp.bfloat16)
    branch = lax.psum_scatter(
        (
            lax.dot_general(
                hidden, down_weight, (((1,), (1,)), ((), ())), preferred_element_type=jnp.float32
            )
            * out_scale
        ).astype(jnp.bfloat16),
        "fs",
        scatter_dimension=0,
        tiled=True,
    ).astype(jnp.float32)
    return (resid_f + 0.5 * branch).astype(jnp.bfloat16)


def on_device(
    prompt,
    norm_first,
    gate_first,
    up_first,
    down_first,
    norm_second,
    gate_second,
    up_second,
    down_second,
):
    first_set = jnp.stack(
        [
            fold_rows(norm_first, gate_first),
            fold_rows(norm_first, up_first),
            down_first.astype(jnp.bfloat16),
        ]
    )
    second_set = jnp.stack(
        [
            fold_rows(norm_second, gate_second),
            fold_rows(norm_second, up_second),
            down_second.astype(jnp.bfloat16),
        ]
    )
    served_first = relayout(first_set)
    middle = half_step(prompt, served_first)
    served_second = relayout(second_set)
    result = half_step(middle, served_second)
    return (
        served_first[0],
        served_first[1],
        served_first[2],
        served_second[0],
        served_second[1],
        served_second[2],
        result,
    )


def solution(mesh):
    in_specs = (
        P(("gr", "fs", "tp"), None),
        P(("gr", "fs")),
        P(("gr", "fs"), "tp"),
        P(("gr", "fs"), "tp"),
        P(("gr", "fs"), "tp"),
        P(("gr", "fs")),
        P(("gr", "fs"), "tp"),
        P(("gr", "fs"), "tp"),
        P(("gr", "fs"), "tp"),
    )
    out_specs = (
        P(None, "fs"),
        P(None, "fs"),
        P(None, "fs"),
        P(None, "fs"),
        P(None, "fs"),
        P(None, "fs"),
        P(("gr", "fs", "tp"), None),
    )
    return jax.shard_map(
        on_device, mesh=mesh, in_specs=in_specs, out_specs=out_specs, check_vma=False
    )
```

profile of v0, /device:TPU:0, one launch (start us, length us, event | category | flops | bytes accessed | tf_op | source)
XLA Modules:
  0.0 607.6 jit_solution(7273351563624397723)
XLA Ops:
  7.2 2.5 fusion.6
  11.8 6.0 all_to_all.72
  17.9 2.6 copy.77
  20.5 10.8 %copy.72 = bf16[3,64,2,2816]{1,0,3,2:T(4,128)(2,1)} copy(bf16[3,64,2,2816]{3,2,1,0:T(2,128)(2,1)S(1)} %bitcast.78) | data formatting | bytes 4325376 | tf_op jit(solution)/shard_map/all_to_all | solution.py:17
  31.3 7.1 %reshape.54 = bf16[8,2,67584]{2,1,0:T(2,128)(2,1)S(1)} reshape(bf16[5632,3,64]{2,1,0:T(4,128)(2,1)} %bitcast.56) | data formatting | bytes 4325376
  38.4 57.7 %all_to_all.73 = bf16[8,2,67584]{2,1,0:T(2,128)(2,1)} all-to-all(bf16[8,2,67584]{2,1,0:T(2,128)(2,1)S(1)} %reshape.54), channel_id=1, replica_groups=mesh['gr'=2,'fs'=8,'tp'=2] {'fs'}, dimensions={0} | all-to-all | bytes 4325376 | tf_op jit(solution)/shard_map/all_to_all | solution.py:16
  96.1 8.0 %reshape.55 = bf16[5632,3,64]{2,1,0:T(4,128)(2,1)} reshape(bf16[8,2,67584]{2,1,0:T(2,128)(2,1)} %all_to_all.73) | data formatting | bytes 4325376
  104.1 9.4 %copy.55 = bf16[3,64,8,704]{3,1,2,0:T(8,128)(2,1)} copy(bf16[3,64,8,704]{1,0,3,2:T(4,128)(2,1)} %bitcast.57) | data formatting | bytes 4325376 | tf_op jit(solution)/shard_map/all_to_all | solution.py:16
  115.0 61.3 %all-gather.5.cloned.1.call-done = bf16[3,2048,704]{2,1,0:T(8,128)(2,1)} async-done(((bf16[3,512,704]{2,1,0:T(8,128)(2,1)}), bf16[3,2048,704]{2,1,0:T(8,128)(2,1)}) %all-gather.5.cloned.1.call-update) | async-done | bytes 8650768 | tf_op jit(solution)/shard_map/all_gather | solution.py:23
  176.3 4.1 fusion.15
  184.5 54.6 %all-gather.9.cloned.1.call-done = bf16[768,2048]{1,0:T(8,128)(2,1)} async-done(((bf16[96,2048]{1,0:T(8,128)(2,1)}), bf16[768,2048]{1,0:T(8,128)(2,1)}) %all-gather.9.cloned.1.call-update) | async-done | bytes 3145744 | tf_op jit(solution)/shard_map/all_gather | solution.py:46
  239.1 5.7 fusion.16
  244.8 12.4 %multiply_convert_fusion.1 = bf16[768,2048]{1,0:T(8,128)(2,1)} fusion(bf16[2048,704]{1,0:T(8,128)(2,1)} %bitcast.64, f32[768,704]{0,1:T(8,128)} %fusion.16, bf16[768,2048]{1,0:T(8,128)(2,1)} %all-gather.9.cloned.1.call-done, bf16[2048,704]{1,0:T(8,128)(2,1)} %bitcast.62), kind=kOutput, calls=%fused_computation.1 | convolution fusion | flops 4436656128 | bytes 14221312 | tf_op jit(solution)/shard_map/dot_general | solution.py:52
  262.5 6.0 all_to_all.74
  268.5 3.9 copy.76
  272.5 15.1 %copy.73 = bf16[3,64,2,2816]{1,0,3,2:T(4,128)(2,1)} copy(bf16[3,64,2,2816]{3,2,1,0:T(2,128)(2,1)} %bitcast.79) | data formatting | bytes 4325376 | tf_op jit(solution)/shard_map/all_to_all | solution.py:17
  287.6 8.2 %reshape.56 = bf16[8,2,67584]{2,1,0:T(2,128)(2,1)} reshape(bf16[5632,3,64]{2,1,0:T(4,128)(2,1)} %bitcast.58) | data formatting | bytes 4325376
  295.9 67.8 %all_to_all.75 = bf16[8,2,67584]{2,1,0:T(2,128)(2,1)} all-to-all(bf16[8,2,67584]{2,1,0:T(2,128)(2,1)} %reshape.56), channel_id=1, replica_groups=mesh['gr'=2,'fs'=8,'tp'=2] {'fs'}, dimensions={0} | all-to-all | bytes 4325376 | tf_op jit(solution)/shard_map/all_to_all | solution.py:16
  363.7 8.0 %reshape.57 = bf16[5632,3,64]{2,1,0:T(4,128)(2,1)} reshape(bf16[8,2,67584]{2,1,0:T(2,128)(2,1)} %all_to_all.75) | data formatting | bytes 4325376
  371.6 9.4 %copy.62 = bf16[3,64,8,704]{3,1,2,0:T(8,128)(2,1)} copy(bf16[3,64,8,704]{1,0,3,2:T(4,128)(2,1)} %bitcast.59) | data formatting | bytes 4325376 | tf_op jit(solution)/shard_map/all_to_all | solution.py:16
  384.5 59.3 %all-gather.7.cloned.1.call-done = bf16[3,2048,704]{2,1,0:T(8,128)(2,1)} async-done(((bf16[3,512,704]{2,1,0:T(8,128)(2,1)}), bf16[3,2048,704]{2,1,0:T(8,128)(2,1)}) %all-gather.7.cloned.1.call-update) | async-done | bytes 8650768 | tf_op jit(solution)/shard_map/all_gather | solution.py:23
  443.8 4.1 fusion.14
  453.6 52.8 %all-gather.11.cloned.1.call-done = bf16[768,2048]{1,0:T(8,128)(2,1)} async-done(((bf16[96,2048]{1,0:T(8,128)(2,1)}), bf16[768,2048]{1,0:T(8,128)(2,1)}) %all-gather.11.cloned.1.call-update) | async-done | bytes 3145744 | tf_op jit(solution)/shard_map/all_gather | solution.py:46
  506.5 6.6 %fusion.17 = f32[768,704]{0,1:T(8,128)} fusion(bf16[768,2048]{1,0:T(8,128)(2,1)} %all-gather.11.cloned.1.call-done, bf16[2048,704]{1,0:T(8,128)(2,1)} %bitcast.66), kind=kOutput, calls=%fused_computation.39 | convolution fusion | flops 2214592512 | bytes 8192000 | tf_op jit(solution)/shard_map/dot_general | solution.py:47
  513.1 12.4 %multiply_convert_fusion = bf16[768,2048]{1,0:T(8,128)(2,1)} fusion(bf16[2048,704]{1,0:T(8,128)(2,1)} %bitcast.70, f32[768,704]{0,1:T(8,128)} %fusion.17, bf16[768,2048]{1,0:T(8,128)(2,1)} %all-gather.11.cloned.1.call-done, bf16[2048,704]{1,0:T(8,128)(2,1)} %bitcast.68), kind=kOutput, calls=%fused_computation | convolution fusion | flops 4436656128 | bytes 14221312 | tf_op jit(solution)/shard_map/dot_general | solution.py:52
  525.6 4.6 copy.69
  530.1 4.6 copy.70
  534.7 4.6 copy.71
  539.2 2.7 copy.66
  541.9 4.7 copy.67
  546.7 2.7 copy.68
  549.3 49.1 %reduce-scatter.5.cloned.1.call-done = bf16[96,2048]{1,0:T(8,128)(2,1)} async-done(((bf16[768,2048]{1,0:T(8,128)(2,1)}), bf16[96,2048]{1,0:T(8,128)(2,1)}) %reduce-scatter.5.cloned.1.call-update) | async-done | bytes 393232 | tf_op jit(solution)/shard_map/reduce_scatter | solution.py:50
  (37 shorter events, 24.1 us)
Async XLA Ops:
  7.2 169.1 %all-gather.5.cloned.1.call-start = ((), (), s32[]{:S(2)}) async-start(), calls=%async_computation.6 | async-start | bytes 11796480 | tf_op jit(solution)/shard_map/all_gather | solution.py:23
  104.1 9.5 %copy-start.1 = (bf16[96,2048]{1,0:T(8,128)(2,1)S(1)}, bf16[96,2048]{1,0:T(8,128)(2,1)}, u32[]{:S(2)}) copy-start(bf16[96,2048]{1,0:T(8,128)(2,1)} %param.9) | copy-start | bytes 1179652
  113.5 125.6 %all-gather.9.cloned.1.call-start = ((), (), s32[]{:S(2)}) async-start(), calls=%async_computation.8 | async-start | bytes 3538944 | tf_op jit(solution)/shard_map/all_gather | solution.py:46
  114.7 266.4 %reduce-scatter.3.cloned.1.call-start = ((), (), s32[]{:S(2)}) async-start(), calls=%async_computation.9 | async-start | bytes 3538944 | tf_op jit(solution)/shard_map/reduce_scatter | solution.py:50
  257.2 0.7 copy-start.2
  257.3 186.5 %all-gather.7.cloned.1.call-start = ((), (), s32[]{:S(2)}) async-start(), calls=%async_computation.7 | async-start | bytes 11796480 | tf_op jit(solution)/shard_map/all_gather | solution.py:23
  381.0 125.4 %all-gather.11.cloned.1.call-start = ((), (), s32[]{:S(2)}) async-start(), calls=%async_computation.10 | async-start | bytes 3538944 | tf_op jit(solution)/shard_map/all_gather | solution.py:46
  384.3 214.2 %reduce-scatter.5.cloned.1.call-start = ((), (), s32[]{:S(2)}) async-start(), calls=%async_computation.11 | async-start | bytes 3538944 | tf_op jit(solution)/shard_map/reduce_scatter | solution.py:50
  541.9 4.7 copy-start
Sparse Core Ops, SparseCore 0:
  113.6 62.6 all-gather.4
  179.1 60.0 all-gather.8
  257.4 96.6 reduce-scatter.2
  381.2 62.5 all-gather.6
  446.4 60.0 all-gather.10
  525.7 72.7 reduce-scatter.4
where the time goes:
time: 615 us; the launch traced here: 608 us
  waiting for transfers between devices  277 us (45%)
  blocking collectives  138 us (22%)
  local copies, waits for them, and re-layouts  128 us (21%)
  matrix products  37.2 us (6%)
  between operations  14.4 us (2%)
  other arithmetic  11.8 us (2%)
    all_to_all x2, blocking collectives, relayout(): lax.all_to_all(lax.all_to_all(stacked, 'tp', split_axis=1, concat_axis=2,...  126 us
    all_gather x2, waiting for transfers between devices, relayout(): whole = lax.all_gather(moved, ('gr', 'tp'), axis=1, tiled=True)  121 us
    all_gather x2, waiting for transfers between devices, half_step(): tokens_in = lax.all_gather(normed, 'fs', axis=0, tiled=True)  107 us
    unnamed x16, local copies, waits for them, and re-layouts  55.2 us
    reduce_scatter x2, waiting for transfers between devices, half_step(): lax.psum_scatter((lax.dot_general(hidden, down_weight, (((1,), (1,)), (()...  49.1 us
    all_to_all x4, local copies, waits for them, and re-layouts, relayout(): lax.all_to_all(stacked, 'tp', split_axis=1, concat_axis=2, tiled=True)  32.4 us
    dot_general x2, matrix products, half_step(): lax.dot_general(hidden, down_weight, (((1,), (1,)), ((), ())), preferred_...  24.9 us
    all_to_all x2, local copies, waits for them, and re-layouts, relayout(): lax.all_to_all(lax.all_to_all(stacked, 'tp', split_axis=1, concat_axis=2,...  18.8 us
  transfers between devices with their start and end apart: 6, of which 5 were waited for; matrix products, arithmetic and copies ran while one was open for 16% of the time, Pallas kernels for 0%

commit v1 on v0

--- a/solution.py
+++ b/solution.py
@@ -43,7 +43,12 @@
     ).astype(jnp.bfloat16)
     in_scale = D ** (-0.5)
     out_scale = FF ** (-0.5)
-    tokens_in = lax.all_gather(normed, "fs", axis=0, tiled=True)
+    ring = [normed]
+    for hop in range(7):
+        ring.append(lax.ppermute(ring[-1], "fs", [(dev, (dev + 1) % 8) for dev in range(8)]))
+    tokens_in = jnp.roll(
+        jnp.concatenate(ring[::-1], axis=0), (lax.axis_index("fs") + 1) * ring[0].shape[0], axis=0
+    )
     gate_pre = jnp.dot(tokens_in, gate_weight, preferred_element_type=jnp.float32) * in_scale
     up_pre = jnp.dot(tokens_in, up_weight, preferred_element_type=jnp.float32) * in_scale
     hidden = (jax.nn.silu(gate_pre) * up_pre).astype(jnp.bfloat16)

time: 615 us -> 549 us (0.89)
  waiting for transfers between devices: 277 us -> 197 us
  local copies, waits for them, and re-layouts: 128 us -> 139 us
    ppermute x0 -> x14, waiting for transfers between devices: none -> 147 us  [half_step(): lax.ppermute(ring[-1], 'fs', [(dev, (dev + 1) % 8) for dev in range(8)])]
    all_gather x2, waiting for transfers between devices: 121 us -> 0.01 us  [relayout(): whole = lax.all_gather(moved, ('gr', 'tp'), axis=1, tiled=True)]
    all_gather x2 -> x0, waiting for transfers between devices: 107 us -> none  [half_step(): tokens_in = lax.all_gather(normed, 'fs', axis=0, tiled=True)]
    unnamed x16 -> x58, local copies, waits for them, and re-layouts: 55.2 us -> 67.6 us
  transfers between devices with their start and end apart: 6 -> 18, of which waited for: 5 -> 15; matrix products, arithmetic and copies ran while one was open for 16% -> 17% of each run, Pallas kernels for 0% -> 0%
where the time goes in v1:
time: 549 us; the launch traced here: 541 us
  waiting for transfers between devices  197 us (36%)
  local copies, waits for them, and re-layouts  139 us (25%)
  blocking collectives  138 us (25%)
  matrix products  38.4 us (7%)
  between operations  14.3 us (3%)
  other arithmetic  11.2 us (2%)
    ppermute x14, waiting for transfers between devices, half_step(): lax.ppermute(ring[-1], 'fs', [(dev, (dev + 1) % 8) for dev in range(8)])  147 us
    all_to_all x2, blocking collectives, relayout(): lax.all_to_all(lax.all_to_all(stacked, 'tp', split_axis=1, concat_axis=2,...  126 us
    unnamed x58, local copies, waits for them, and re-layouts  67.6 us
    reduce_scatter x2, waiting for transfers between devices, half_step(): lax.psum_scatter((lax.dot_general(hidden, down_weight, (((1,), (1,)), (()...  49.8 us
    all_to_all x4, local copies, waits for them, and re-layouts, relayout(): lax.all_to_all(stacked, 'tp', split_axis=1, concat_axis=2, tiled=True)  32.5 us
    dot_general x2, matrix products, half_step(): lax.dot_general(hidden, down_weight, (((1,), (1,)), ((), ())), preferred_...  26.7 us
    all_to_all x2, local copies, waits for them, and re-layouts, relayout(): lax.all_to_all(lax.all_to_all(stacked, 'tp', split_axis=1, concat_axis=2,...  18.8 us
    all_to_all x2, blocking collectives, relayout(): lax.all_to_all(stacked, 'tp', split_axis=1, concat_axis=2, tiled=True)  12.1 us
  transfers between devices with their start and end apart: 18, of which 15 were waited for; matrix products, arithmetic and copies ran while one was open for 17% of the time, Pallas kernels for 0%

profile of v1, /device:TPU:0, one launch (start us, length us, event | category | flops | bytes accessed | tf_op | source)
XLA Modules:
  0.0 540.6 jit_solution(12292680967409115006)
XLA Ops:
  11.8 6.0 %all_to_all.72 = bf16[3,128,2816]{2,0,1:T(4,128)(2,1)S(1)} all-to-all(bf16[3,128,2816]{2,0,1:T(4,128)(2,1)S(1)} %copy.52), channel_id=1, replica_groups=mesh['gr'=2,'fs'=8,'tp'=2] {'tp'}, dimensions={1} | all-to-all | bytes 4325376 | tf_op jit(solution)/shard_map/all_to_all | solution.py:17
  20.5 10.8 %copy.72 = bf16[3,64,2,2816]{1,0,3,2:T(4,128)(2,1)} copy(bf16[3,64,2,2816]{3,2,1,0:T(2,128)(2,1)S(1)} %bitcast.74) | data formatting | bytes 4325376 | tf_op jit(solution)/shard_map/all_to_all | solution.py:17
  31.3 7.1 %reshape.54 = bf16[8,2,67584]{2,1,0:T(2,128)(2,1)S(1)} reshape(bf16[5632,3,64]{2,1,0:T(4,128)(2,1)} %bitcast.52) | data formatting | bytes 4325376
  38.4 57.7 %all_to_all.73 = bf16[8,2,67584]{2,1,0:T(2,128)(2,1)} all-to-all(bf16[8,2,67584]{2,1,0:T(2,128)(2,1)S(1)} %reshape.54), channel_id=1, replica_groups=mesh['gr'=2,'fs'=8,'tp'=2] {'fs'}, dimensions={0} | all-to-all | bytes 4325376 | tf_op jit(solution)/shard_map/all_to_all | solution.py:16
  96.2 7.9 %reshape.55 = bf16[5632,3,64]{2,1,0:T(4,128)(2,1)} reshape(bf16[8,2,67584]{2,1,0:T(2,128)(2,1)} %all_to_all.73) | data formatting | bytes 4325376
  104.1 9.4 %copy.55 = bf16[3,64,8,704]{3,1,2,0:T(8,128)(2,1)} copy(bf16[3,64,8,704]{1,0,3,2:T(4,128)(2,1)} %bitcast.53) | data formatting | bytes 4325376 | tf_op jit(solution)/shard_map/all_to_all | solution.py:16
  114.8 11.5 %collective-permute-done = bf16[96,2048]{1,0:T(8,128)(2,1)S(1)} collective-permute-done((bf16[96,2048]{1,0:T(8,128)(2,1)S(1)}, bf16[96,2048]{1,0:T(8,128)(2,1)S(1)}, u32[]{:S(2)}, u32[]{:S(2)}) %collective-permute-start) | collective-permute-done | bytes 393248 | tf_op jit(solution)/shard_map/ppermute | solution.py:48
  126.3 11.4 %collective-permute-done.1 = bf16[96,2048]{1,0:T(8,128)(2,1)S(1)} collective-permute-done((bf16[96,2048]{1,0:T(8,128)(2,1)S(1)}, bf16[96,2048]{1,0:T(8,128)(2,1)S(1)}, u32[]{:S(2)}, u32[]{:S(2)}) %collective-permute-start.1) | collective-permute-done | bytes 393248 | tf_op jit(solution)/shard_map/ppermute | solution.py:48
  137.7 10.6 %collective-permute-done.2 = bf16[96,2048]{1,0:T(8,128)(2,1)S(1)} collective-permute-done((bf16[96,2048]{1,0:T(8,128)(2,1)S(1)}, bf16[96,2048]{1,0:T(8,128)(2,1)S(1)}, u32[]{:S(2)}, u32[]{:S(2)}) %collective-permute-start.2) | collective-permute-done | bytes 393248 | tf_op jit(solution)/shard_map/ppermute | solution.py:48
  148.3 10.5 %collective-permute-done.3 = bf16[96,2048]{1,0:T(8,128)(2,1)S(1)} collective-permute-done((bf16[96,2048]{1,0:T(8,128)(2,1)S(1)}, bf16[96,2048]{1,0:T(8,128)(2,1)S(1)}, u32[]{:S(2)}, u32[]{:S(2)}) %collective-permute-start.3) | collective-permute-done | bytes 393248 | tf_op jit(solution)/shard_map/ppermute | solution.py:48
  158.7 11.5 %collective-permute-done.4 = bf16[96,2048]{1,0:T(8,128)(2,1)S(1)} collective-permute-done((bf16[96,2048]{1,0:T(8,128)(2,1)S(1)}, bf16[96,2048]{1,0:T(8,128)(2,1)S(1)}, u32[]{:S(2)}, u32[]{:S(2)}) %collective-permute-start.4) | collective-permute-done | bytes 393248 | tf_op jit(solution)/shard_map/ppermute | solution.py:48
  170.2 12.2 %collective-permute-done.5 = bf16[96,2048]{1,0:T(8,128)(2,1)S(1)} collective-permute-done((bf16[96,2048]{1,0:T(8,128)(2,1)S(1)}, bf16[96,2048]{1,0:T(8,128)(2,1)S(1)}, u32[]{:S(2)}, u32[]{:S(2)}) %collective-permute-start.5) | collective-permute-done | bytes 393248 | tf_op jit(solution)/shard_map/ppermute | solution.py:48
  182.9 10.4 %collective-permute-done.6 = bf16[96,2048]{1,0:T(8,128)(2,1)S(1)} collective-permute-done((bf16[96,2048]{1,0:T(8,128)(2,1)S(1)}, bf16[96,2048]{1,0:T(8,128)(2,1)S(1)}, u32[]{:S(2)}, u32[]{:S(2)}) %collective-permute-start.6) | collective-permute-done | bytes 393248 | tf_op jit(solution)/shard_map/ppermute | solution.py:48
  207.9 6.6 %fusion.16 = f32[768,704]{0,1:T(8,128)} fusion(bf16[2048,704]{1,0:T(8,128)(2,1)S(1)} %bitcast.56, s32[]{:T(128)S(6)} %select_n.13, bf16[768,2048]{1,0:T(8,128)(2,1)} %constant_dynamic-update-slice_fusion), kind=kOutput, calls=%fused_computation.58 | convolution fusion | flops 2220883968 | bytes 8192004 | tf_op jit(solution)/shard_map/dot_general | solution.py:52
  214.4 13.3 %multiply_convert_fusion.1 = bf16[768,2048]{1,0:T(8,128)(2,1)} fusion(bf16[2048,704]{1,0:T(8,128)(2,1)} %bitcast.60, f32[768,704]{0,1:T(8,128)} %fusion.16, bf16[2048,704]{1,0:T(8,128)(2,1)} %bitcast.58, s32[]{:T(128)S(6)} %select_n.13, bf16[768,2048]{1,0:T(8,128)(2,1)} %constant_dynamic-update-slice_fusion), kind=kOutput, calls=%fused_computation.5 | convolution fusion | flops 4442947584 | bytes 14221316 | tf_op jit(solution)/shard_map/dot_general | solution.py:57
  233.0 6.0 %all_to_all.74 = bf16[3,128,2816]{2,0,1:T(4,128)(2,1)S(1)} all-to-all(bf16[3,128,2816]{2,0,1:T(4,128)(2,1)S(1)} %copy.59), channel_id=1, replica_groups=mesh['gr'=2,'fs'=8,'tp'=2] {'tp'}, dimensions={1} | all-to-all | bytes 4325376 | tf_op jit(solution)/shard_map/all_to_all | solution.py:17
  243.0 15.1 %copy.73 = bf16[3,64,2,2816]{1,0,3,2:T(4,128)(2,1)} copy(bf16[3,64,2,2816]{3,2,1,0:T(2,128)(2,1)} %bitcast.75) | data formatting | bytes 4325376 | tf_op jit(solution)/shard_map/all_to_all | solution.py:17
  258.1 8.2 %reshape.56 = bf16[8,2,67584]{2,1,0:T(2,128)(2,1)} reshape(bf16[5632,3,64]{2,1,0:T(4,128)(2,1)} %bitcast.54) | data formatting | bytes 4325376
  266.4 67.8 %all_to_all.75 = bf16[8,2,67584]{2,1,0:T(2,128)(2,1)} all-to-all(bf16[8,2,67584]{2,1,0:T(2,128)(2,1)} %reshape.56), channel_id=1, replica_groups=mesh['gr'=2,'fs'=8,'tp'=2] {'fs'}, dimensions={0} | all-to-all | bytes 4325376 | tf_op jit(solution)/shard_map/all_to_all | solution.py:16
  334.2 7.9 %reshape.57 = bf16[5632,3,64]{2,1,0:T(4,128)(2,1)} reshape(bf16[8,2,67584]{2,1,0:T(2,128)(2,1)} %all_to_all.75) | data formatting | bytes 4325376
  342.1 9.4 %copy.62 = bf16[3,64,8,704]{3,1,2,0:T(8,128)(2,1)} copy(bf16[3,64,8,704]{1,0,3,2:T(4,128)(2,1)} %bitcast.55) | data formatting | bytes 4325376 | tf_op jit(solution)/shard_map/all_to_all | solution.py:16
  355.6 11.6 %collective-permute-done.7 = bf16[96,2048]{1,0:T(8,128)(2,1)S(1)} collective-permute-done((bf16[96,2048]{1,0:T(8,128)(2,1)S(1)}, bf16[96,2048]{1,0:T(8,128)(2,1)S(1)}, u32[]{:S(2)}, u32[]{:S(2)}) %collective-permute-start.7) | collective-permute-done | bytes 393248 | tf_op jit(solution)/shard_map/ppermute | solution.py:48
  368.0 11.6 %collective-permute-done.8 = bf16[96,2048]{1,0:T(8,128)(2,1)S(1)} collective-permute-done((bf16[96,2048]{1,0:T(8,128)(2,1)S(1)}, bf16[96,2048]{1,0:T(8,128)(2,1)S(1)}, u32[]{:S(2)}, u32[]{:S(2)}) %collective-permute-start.8) | collective-permute-done | bytes 393248 | tf_op jit(solution)/shard_map/ppermute | solution.py:48
  380.3 10.7 %collective-permute-done.9 = bf16[96,2048]{1,0:T(8,128)(2,1)S(1)} collective-permute-done((bf16[96,2048]{1,0:T(8,128)(2,1)S(1)}, bf16[96,2048]{1,0:T(8,128)(2,1)S(1)}, u32[]{:S(2)}, u32[]{:S(2)}) %collective-permute-start.9) | collective-permute-done | bytes 393248 | tf_op jit(solution)/shard_map/ppermute | solution.py:48
  391.8 10.5 %collective-permute-done.10 = bf16[96,2048]{1,0:T(8,128)(2,1)S(1)} collective-permute-done((bf16[96,2048]{1,0:T(8,128)(2,1)S(1)}, bf16[96,2048]{1,0:T(8,128)(2,1)S(1)}, u32[]{:S(2)}, u32[]{:S(2)}) %collective-permute-start.10) | collective-permute-done | bytes 393248 | tf_op jit(solution)/shard_map/ppermute | solution.py:48
  403.0 10.6 %collective-permute-done.11 = bf16[96,2048]{1,0:T(8,128)(2,1)S(1)} collective-permute-done((bf16[96,2048]{1,0:T(8,128)(2,1)S(1)}, bf16[96,2048]{1,0:T(8,128)(2,1)S(1)}, u32[]{:S(2)}, u32[]{:S(2)}) %collective-permute-start.11) | collective-permute-done | bytes 393248 | tf_op jit(solution)/shard_map/ppermute | solution.py:48
  414.3 12.2 %collective-permute-done.12 = bf16[96,2048]{1,0:T(8,128)(2,1)} collective-permute-done((bf16[96,2048]{1,0:T(8,128)(2,1)S(1)}, bf16[96,2048]{1,0:T(8,128)(2,1)}, u32[]{:S(2)}, u32[]{:S(2)}) %collective-permute-start.12) | collective-permute-done | bytes 393248 | tf_op jit(solution)/shard_map/ppermute | solution.py:48
  439.7 5.1 fusion.20
  444.9 13.3 %multiply_convert_fusion = bf16[768,2048]{1,0:T(8,128)(2,1)} fusion(bf16[2048,704]{1,0:T(8,128)(2,1)} %bitcast.66, f32[768,704]{0,1:T(8,128)} %fusion.20, bf16[2048,704]{1,0:T(8,128)(2,1)} %bitcast.64, s32[]{:T(128)S(6)} %select_n.13, bf16[768,2048]{1,0:T(8,128)(2,1)} %copy-done.15), kind=kOutput, calls=%fused_computation.4 | convolution fusion | flops 4442947584 | bytes 14221316 | tf_op jit(solution)/shard_map/dot_general | solution.py:57
  467.4 4.6 copy.71
  474.6 4.7 copy.67
  482.0 49.8 %reduce-scatter.5.cloned.1.call-done = bf16[96,2048]{1,0:T(8,128)(2,1)} async-done(((bf16[768,2048]{1,0:T(8,128)(2,1)}), bf16[96,2048]{1,0:T(8,128)(2,1)}) %reduce-scatter.5.cloned.1.call-update) | async-done | bytes 393232 | tf_op jit(solution)/shard_map/reduce_scatter | solution.py:55
  (103 shorter events, 70.1 us)
Async XLA Ops:
  7.2 192.5 %all-gather.3.cloned.1.call-start = ((), (), s32[]{:S(2)}) async-start(), calls=%async_computation.6 | async-start | bytes 11796480 | tf_op jit(solution)/shard_map/all_gather | solution.py:23
  104.1 9.5 %copy-start = (bf16[96,2048]{1,0:T(8,128)(2,1)S(1)}, bf16[96,2048]{1,0:T(8,128)(2,1)}, u32[]{:S(2)}) copy-start(bf16[96,2048]{1,0:T(8,128)(2,1)} %param.11) | copy-start | bytes 1179652
  113.5 238.1 %reduce-scatter.3.cloned.1.call-start = ((), (), s32[]{:S(2)}) async-start(), calls=%async_computation.8 | async-start | bytes 3538944 | tf_op jit(solution)/shard_map/reduce_scatter | solution.py:55
  113.9 12.3 %collective-permute-start = (bf16[96,2048]{1,0:T(8,128)(2,1)S(1)}, bf16[96,2048]{1,0:T(8,128)(2,1)S(1)}, u32[]{:S(2)}, u32[]{:S(2)}) collective-permute-start(bf16[96,2048]{1,0:T(8,128)(2,1)S(1)} %fusion.3), channel_id=1, source_target_pairs={{0,2},{2,4},{4,6},{6,8},{8,10},{10,12},{12,14},{14,0},{1,3},{3,5},... | collective-permute-start | bytes 1179656 | tf_op jit(solution)/shard_map/ppermute | solution.py:48
  126.3 11.4 %collective-permute-start.1 = (bf16[96,2048]{1,0:T(8,128)(2,1)S(1)}, bf16[96,2048]{1,0:T(8,128)(2,1)S(1)}, u32[]{:S(2)}, u32[]{:S(2)}) collective-permute-start(bf16[96,2048]{1,0:T(8,128)(2,1)S(1)} %collective-permute-done), channel_id=1, source_target_pairs={{0,2},{2,4},{4,6},{6,8},{8,10},{10,12},{12,14},{14,0},{1,3},{3,5},... | collective-permute-start | bytes 1179656 | tf_op jit(solution)/shard_map/ppermute | solution.py:48
  137.7 10.6 %collective-permute-start.2 = (bf16[96,2048]{1,0:T(8,128)(2,1)S(1)}, bf16[96,2048]{1,0:T(8,128)(2,1)S(1)}, u32[]{:S(2)}, u32[]{:S(2)}) collective-permute-start(bf16[96,2048]{1,0:T(8,128)(2,1)S(1)} %collective-permute-done.1), channel_id=1, source_target_pairs={{0,2},{2,4},{4,6},{6,8},{8,10},{10,12},{12,14},{14,0},{1,3},{3,5},... | collective-permute-start | bytes 1179656 | tf_op jit(solution)/shard_map/ppermute | solution.py:48
  148.3 10.5 %collective-permute-start.3 = (bf16[96,2048]{1,0:T(8,128)(2,1)S(1)}, bf16[96,2048]{1,0:T(8,128)(2,1)S(1)}, u32[]{:S(2)}, u32[]{:S(2)}) collective-permute-start(bf16[96,2048]{1,0:T(8,128)(2,1)S(1)} %collective-permute-done.2), channel_id=1, source_target_pairs={{0,2},{2,4},{4,6},{6,8},{8,10},{10,12},{12,14},{14,0},{1,3},{3,5},... | collective-permute-start | bytes 1179656 | tf_op jit(solution)/shard_map/ppermute | solution.py:48
  158.7 11.5 %collective-permute-start.4 = (bf16[96,2048]{1,0:T(8,128)(2,1)S(1)}, bf16[96,2048]{1,0:T(8,128)(2,1)S(1)}, u32[]{:S(2)}, u32[]{:S(2)}) collective-permute-start(bf16[96,2048]{1,0:T(8,128)(2,1)S(1)} %collective-permute-done.3), channel_id=1, source_target_pairs={{0,2},{2,4},{4,6},{6,8},{8,10},{10,12},{12,14},{14,0},{1,3},{3,5},... | collective-permute-start | bytes 1179656 | tf_op jit(solution)/shard_map/ppermute | solution.py:48
  170.2 12.2 %collective-permute-start.5 = (bf16[96,2048]{1,0:T(8,128)(2,1)S(1)}, bf16[96,2048]{1,0:T(8,128)(2,1)S(1)}, u32[]{:S(2)}, u32[]{:S(2)}) collective-permute-start(bf16[96,2048]{1,0:T(8,128)(2,1)S(1)} %collective-permute-done.4), channel_id=1, source_target_pairs={{0,2},{2,4},{4,6},{6,8},{8,10},{10,12},{12,14},{14,0},{1,3},{3,5},... | collective-permute-start | bytes 1179656 | tf_op jit(solution)/shard_map/ppermute | solution.py:48
  182.4 10.9 %collective-permute-start.6 = (bf16[96,2048]{1,0:T(8,128)(2,1)S(1)}, bf16[96,2048]{1,0:T(8,128)(2,1)S(1)}, u32[]{:S(2)}, u32[]{:S(2)}) collective-permute-start(bf16[96,2048]{1,0:T(8,128)(2,1)S(1)} %collective-permute-done.5), channel_id=1, source_target_pairs={{0,2},{2,4},{4,6},{6,8},{8,10},{10,12},{12,14},{14,0},{1,3},{3,5},... | collective-permute-start | bytes 1179656 | tf_op jit(solution)/shard_map/ppermute | solution.py:48
  227.8 198.8 %all-gather.5.cloned.1.call-start = ((), (), s32[]{:S(2)}) async-start(), calls=%async_computation.7 | async-start | bytes 11796480 | tf_op jit(solution)/shard_map/all_gather | solution.py:23
  351.5 180.3 %reduce-scatter.5.cloned.1.call-start = ((), (), s32[]{:S(2)}) async-start(), calls=%async_computation.9 | async-start | bytes 3538944 | tf_op jit(solution)/shard_map/reduce_scatter | solution.py:55
  354.0 0.7 copy-start.3
  354.8 12.5 %collective-permute-start.7 = (bf16[96,2048]{1,0:T(8,128)(2,1)S(1)}, bf16[96,2048]{1,0:T(8,128)(2,1)S(1)}, u32[]{:S(2)}, u32[]{:S(2)}) collective-permute-start(bf16[96,2048]{1,0:T(8,128)(2,1)S(1)} %fusion.6), channel_id=1, source_target_pairs={{0,2},{2,4},{4,6},{6,8},{8,10},{10,12},{12,14},{14,0},{1,3},{3,5},... | collective-permute-start | bytes 1179656 | tf_op jit(solution)/shard_map/ppermute | solution.py:48
  367.2 0.7 copy-start.5
  368.0 11.6 %collective-permute-start.8 = (bf16[96,2048]{1,0:T(8,128)(2,1)S(1)}, bf16[96,2048]{1,0:T(8,128)(2,1)S(1)}, u32[]{:S(2)}, u32[]{:S(2)}) collective-permute-start(bf16[96,2048]{1,0:T(8,128)(2,1)S(1)} %collective-permute-done.7), channel_id=1, source_target_pairs={{0,2},{2,4},{4,6},{6,8},{8,10},{10,12},{12,14},{14,0},{1,3},{3,5},... | collective-permute-start | bytes 1179656 | tf_op jit(solution)/shard_map/ppermute | solution.py:48
  379.6 0.7 copy-start.7
  380.3 10.7 %collective-permute-start.9 = (bf16[96,2048]{1,0:T(8,128)(2,1)S(1)}, bf16[96,2048]{1,0:T(8,128)(2,1)S(1)}, u32[]{:S(2)}, u32[]{:S(2)}) collective-permute-start(bf16[96,2048]{1,0:T(8,128)(2,1)S(1)} %collective-permute-done.8), channel_id=1, source_target_pairs={{0,2},{2,4},{4,6},{6,8},{8,10},{10,12},{12,14},{14,0},{1,3},{3,5},... | collective-permute-start | bytes 1179656 | tf_op jit(solution)/shard_map/ppermute | solution.py:48
  391.8 10.5 %collective-permute-start.10 = (bf16[96,2048]{1,0:T(8,128)(2,1)S(1)}, bf16[96,2048]{1,0:T(8,128)(2,1)S(1)}, u32[]{:S(2)}, u32[]{:S(2)}) collective-permute-start(bf16[96,2048]{1,0:T(8,128)(2,1)S(1)} %collective-permute-done.9), channel_id=1, source_target_pairs={{0,2},{2,4},{4,6},{6,8},{8,10},{10,12},{12,14},{14,0},{1,3},{3,5},... | collective-permute-start | bytes 1179656 | tf_op jit(solution)/shard_map/ppermute | solution.py:48
  403.0 10.6 %collective-permute-start.11 = (bf16[96,2048]{1,0:T(8,128)(2,1)S(1)}, bf16[96,2048]{1,0:T(8,128)(2,1)S(1)}, u32[]{:S(2)}, u32[]{:S(2)}) collective-permute-start(bf16[96,2048]{1,0:T(8,128)(2,1)S(1)} %collective-permute-done.10), channel_id=1, source_target_pairs={{0,2},{2,4},{4,6},{6,8},{8,10},{10,12},{12,14},{14,0},{1,3},{3,5},... | collective-permute-start | bytes 1179656 | tf_op jit(solution)/shard_map/ppermute | solution.py:48
  413.6 0.7 copy-start.13
  414.3 12.3 %collective-permute-start.12 = (bf16[96,2048]{1,0:T(8,128)(2,1)S(1)}, bf16[96,2048]{1,0:T(8,128)(2,1)}, u32[]{:S(2)}, u32[]{:S(2)}) collective-permute-start(bf16[96,2048]{1,0:T(8,128)(2,1)S(1)} %collective-permute-done.11), channel_id=1, source_target_pairs={{0,2},{2,4},{4,6},{6,8},{8,10},{10,12},{12,14},{14,0},{1,3},{3,5},... | collective-permute-start | bytes 1179656 | tf_op jit(solution)/shard_map/ppermute | solution.py:48
  426.6 10.8 %collective-permute-start.13 = (bf16[96,2048]{1,0:T(8,128)(2,1)}, bf16[96,2048]{1,0:T(8,128)(2,1)}, u32[]{:S(2)}, u32[]{:S(2)}) collective-permute-start(bf16[96,2048]{1,0:T(8,128)(2,1)} %collective-permute-done.12), channel_id=1, source_target_pairs={{0,2},{2,4},{4,6},{6,8},{8,10},{10,12},{12,14},{14,0},{1,3},{3,5},... | collective-permute-start | bytes 1179656 | tf_op jit(solution)/shard_map/ppermute | solution.py:48
  431.2 8.5 %copy-start.2 = (bf16[1,2,8,2,64,704]{5,4,3,2,1,0:T(8,128)(2,1)}, bf16[1,2,8,2,64,704]{5,4,3,2,1,0:T(8,128)(2,1)S(1)}, u32[]{:S(2)}) copy-start(bf16[1,2,8,2,64,704]{5,4,3,2,1,0:T(8,128)(2,1)S(1)} %copy.63) | copy-start | bytes 8650756
  433.3 6.1 %copy-start.14 = (bf16[96,2048]{1,0:T(8,128)(2,1)S(1)}, bf16[96,2048]{1,0:T(8,128)(2,1)}, u32[]{:S(2)}) copy-start(bf16[96,2048]{1,0:T(8,128)(2,1)} %copy-done.13) | copy-start | bytes 1179652
  433.3 6.2 %copy-start.12 = (bf16[96,2048]{1,0:T(8,128)(2,1)S(1)}, bf16[96,2048]{1,0:T(8,128)(2,1)}, u32[]{:S(2)}) copy-start(bf16[96,2048]{1,0:T(8,128)(2,1)} %copy-done.11) | copy-start | bytes 1179652
  433.3 6.2 %copy-start.10 = (bf16[96,2048]{1,0:T(8,128)(2,1)S(1)}, bf16[96,2048]{1,0:T(8,128)(2,1)}, u32[]{:S(2)}) copy-start(bf16[96,2048]{1,0:T(8,128)(2,1)} %copy-done.9) | copy-start | bytes 1179652
  435.2 4.3 copy-start.8
  435.2 4.4 copy-start.6
  435.2 4.4 copy-start.4
  439.7 5.2 copy-start.15
  474.6 4.7 copy-start.1
  (3 other events, 2.1 us)
Sparse Core Ops, SparseCore 0:
  113.7 62.6 all-gather.2
  227.9 91.3 reduce-scatter.2
  351.6 62.5 all-gather.4
  458.3 73.4 reduce-scatter.4
